TPU v7x, 32 devices: a whole 2x2x4 slice. The times are simulated.
32 devices in a mesh: ep: 4 (over y, x), tp: 8 (over z, core).
Axes of the slice: x: 2, y: 2, z: 4, core: 2. Of those that a mesh axis runs over, the one named last changes fastest.
Arguments:
- mix_tokens: bfloat16 [2048, 1, 1024], P(('ep', 'tp')), may hold values from -6 to 6
- mix_gain: float32 [1024], replicated, may hold values from 0.1 to 1.9
- w_query: bfloat16 [1024, 1024], replicated, may hold values from -0.1875 to 0.1875
- w_key: bfloat16 [1024, 256], replicated, may hold values from -0.1875 to 0.1875
- w_value: bfloat16 [1024, 256], replicated, may hold values from -0.1875 to 0.1875
- query_gain: float32 [64], replicated, may hold values from 1.2 to 14
- key_gain: float32 [64], replicated, may hold values from 1.2 to 14
- w_out: bfloat16 [1024, 1024], replicated, may hold values from -0.1875 to 0.1875
- expert_tokens: bfloat16 [4096, 1024], P(('ep', 'tp')), may hold values from -6 to 6
- expert_gain: float32 [1024], replicated, may hold values from 0.1 to 1.9
- route_ids: int32 [4096, 2], P(('ep', 'tp')), may hold values from 0 to 7, all different within a row; in each aligned block of 128 rows (0 to 127, 128 to 255, ...) at most 36 rows name the same one
- route_weights: float32 [4096, 2], P(('ep', 'tp')), may hold values from 0.1 to 1
- w_gate: bfloat16 [8, 1024, 4096], P('ep', None, 'tp'), may hold values from -0.1875 to 0.1875
- w_up: bfloat16 [8, 1024, 4096], P('ep', None, 'tp'), may hold values from -0.1875 to 0.1875
- w_down: bfloat16 [8, 4096, 1024], P('ep', 'tp'), may hold values from -0.09375 to 0.09375
Outputs:
- mix_out: bfloat16 [2048, 1, 1024], P(('ep', 'tp'))
- experts_out: bfloat16 [4096, 1024], P(('ep', 'tp'))
Inputs may be any that keep to these rules, and one draw needn't show every extreme that they name: `route_ids`: each row names 2 different experts. Among the rows of one device no expert is named more than 36 times, and in every draw some expert is named exactly 36 times by the rows of some device.
All inputs are finite; a program needn't handle non-finite values.
Results may differ from a plain program's by a relative error of at most 0.018.
The roundings to bfloat16 on the way count: a program that leaves them out, or rounds other values in their place, can miss the bound.
Values may be sent and summed in bfloat16 or wider, within the bound.
No kernel may reach another device: no remote copies, remote signals or barrier semaphores. Data moves between devices by JAX's collectives and lax.ppermute only.
A program may use at most 128 MiB of HBM per device.

v0:
```python
import math

import jax
import jax.numpy as jnp
from jax import lax
from jax.sharding import PartitionSpec as P

HEAD = 64
GRID_W = 64


epsilon = 1e-06


def normalize(values, gain_vec):
    widened = values.astype(jnp.float32)
    return (
        widened
        * lax.rsqrt(jnp.mean(widened * widened, axis=-1, keepdims=True) + epsilon)
        * gain_vec
    )


def angle_tables(positions, head_size):
    quarter = head_size // 4
    frequency = 10000.0 ** (-jnp.arange(quarter, dtype=jnp.float32) / quarter)
    grid_pos = jnp.stack([positions // GRID_W, positions % GRID_W], axis=-1).astype(jnp.float32)
    angles = grid_pos[:, :, None] * frequency[None, None, :]
    return (jnp.cos(angles), jnp.sin(angles))


def turn(values, cosine_table, sine_table):
    shaped = values.shape
    quarter = shaped[-1] // 4
    leading = (shaped[0],) + (1,) * (len(shaped) - 2) + (2, quarter)
    cosine_table = cosine_table.reshape(leading)
    sine_table = sine_table.reshape(leading)
    halves = values.reshape(shaped[:-1] + (2, 2, quarter))
    first_part = halves[..., 0, :]
    second_part = halves[..., 1, :]
    turned = jnp.stack(
        [
            first_part * cosine_table - second_part * sine_table,
            first_part * sine_table + second_part * cosine_table,
        ],
        axis=-2,
    )
    return turned.reshape(shaped)


def attend(queries, fold_state, key_piece):
    key_rows = key_piece.shape[0]
    block_rows = math.gcd(key_rows, 1024)
    blocks = key_piece.reshape((key_rows // block_rows, block_rows) + key_piece.shape[1:])
    score_scale = HEAD ** (-0.5)

    def step_block(carried, block_keys):
        running_max, totals, accumulated = carried
        keys_part = block_keys[..., :HEAD]
        values_part = block_keys[..., HEAD:]
        scores = (
            jnp.einsum("qshd,ksd->qshk", queries, keys_part, preferred_element_type=jnp.float32)
            * score_scale
        )
        new_max = jnp.maximum(running_max, jnp.max(scores, axis=-1))
        shrink = jnp.exp(running_max - new_max)
        raised = jnp.exp(scores - new_max[..., None])
        totals = totals * shrink + jnp.sum(raised, axis=-1)
        accumulated = accumulated * shrink[..., None] + jnp.einsum(
            "qshk,ksd->qshd",
            raised.astype(jnp.bfloat16),
            values_part,
            preferred_element_type=jnp.float32,
        )
        return ((new_max, totals, accumulated), None)

    return lax.scan(step_block, fold_state, blocks)[0]


def mixer_half(mix_tokens, mix_gain, w_query, w_key, w_value, query_gain, key_gain, w_out):
    tp_count = lax.axis_size("tp")
    seq_rows, sequences, model_width = mix_tokens.shape
    head_count = w_query.shape[1] // HEAD
    key_heads = w_key.shape[1] // HEAD
    local_heads = head_count // tp_count
    normed = normalize(mix_tokens, mix_gain).astype(jnp.bfloat16)
    queries = jnp.dot(normed, w_query, preferred_element_type=jnp.float32).astype(jnp.bfloat16)
    keys_raw = jnp.dot(normed, w_key, preferred_element_type=jnp.float32).astype(jnp.bfloat16)
    values = jnp.dot(normed, w_value, preferred_element_type=jnp.float32).astype(jnp.bfloat16)
    queries = queries.reshape(seq_rows, sequences, tp_count, local_heads * HEAD)
    key_value = jnp.concatenate(
        [
            keys_raw.reshape(seq_rows, sequences, key_heads, HEAD),
            values.reshape(seq_rows, sequences, key_heads, HEAD),
        ],
        axis=-1,
    )
    key_value = jnp.repeat(key_value, tp_count // key_heads, axis=2)
    packed = jnp.concatenate([queries, key_value], axis=-1)
    arrived = lax.all_to_all(packed, "tp", split_axis=2, concat_axis=0, tiled=True)
    span_rows = arrived.shape[0]
    positions = lax.axis_index("ep") * span_rows + jnp.arange(span_rows, dtype=jnp.int32)
    cosine_table, sine_table = angle_tables(positions, HEAD)
    query_width = local_heads * HEAD
    own_queries = normalize(
        arrived[:, :, 0, :query_width].reshape(span_rows, sequences, local_heads, HEAD), query_gain
    )
    own_queries = turn(own_queries, cosine_table, sine_table).astype(jnp.bfloat16)
    own_keys = normalize(arrived[:, :, 0, query_width : query_width + HEAD], key_gain)
    own_keys = turn(own_keys, cosine_table, sine_table).astype(jnp.bfloat16)
    key_pairs = jnp.concatenate([own_keys, arrived[:, :, 0, query_width + HEAD :]], axis=-1)
    start_state = (
        jnp.full((span_rows, sequences, local_heads), -1e30, jnp.float32),
        jnp.zeros((span_rows, sequences, local_heads), jnp.float32),
        jnp.zeros((span_rows, sequences, local_heads, HEAD), jnp.float32),
    )
    running_max, totals, accumulated = attend(
        own_queries, start_state, lax.all_gather(key_pairs, "ep", axis=0, tiled=True)
    )
    mixed = (
        (accumulated / totals[..., None])
        .astype(jnp.bfloat16)
        .reshape(span_rows, sequences, query_width)
    )
    returned = lax.all_to_all(mixed, "tp", split_axis=0, concat_axis=2, tiled=True)
    return jnp.dot(returned, w_out, preferred_element_type=jnp.float32).astype(jnp.bfloat16)


def joint_hidden(w_gate, w_up, piece_rows):
    gate_act = jnp.einsum("rjd,jdf->rjf", piece_rows, w_gate, preferred_element_type=jnp.float32)
    up_act = jnp.einsum("rjd,jdf->rjf", piece_rows, w_up, preferred_element_type=jnp.float32)
    return (jax.nn.silu(gate_act) * up_act).astype(jnp.bfloat16)


def joint_down(hidden_all, w_down):
    group_sum = jnp.einsum(
        "rjf,jfd->rjd", hidden_all, w_down, preferred_element_type=jnp.float32
    ).astype(jnp.bfloat16)
    return lax.optimization_barrier(group_sum).astype(jnp.float32)


def expert_half(expert_tokens, expert_gain, route_ids, route_weights, w_gate, w_up, w_down):
    ep_count = lax.axis_size("ep")
    tok_count, model_width = expert_tokens.shape
    top_count = route_ids.shape[1]
    local_experts = w_gate.shape[0]
    expert_count = local_experts * ep_count
    capacity = tok_count * top_count * 9 // (8 * expert_count)
    slot_count = ep_count * capacity * local_experts
    normed = normalize(expert_tokens, expert_gain).astype(jnp.bfloat16)
    flat_ids = route_ids.reshape(-1)
    matches = (flat_ids[:, None] == jnp.arange(expert_count, dtype=jnp.int32)[None, :]).astype(
        jnp.int32
    )
    rank_ids = jnp.sum((jnp.cumsum(matches, axis=0) - 1) * matches, axis=1)
    slot_ids = (
        flat_ids // local_experts * capacity + rank_ids
    ) * local_experts + flat_ids % local_experts
    chosen = slot_ids.reshape(tok_count, top_count)
    dispatch = jnp.sum(
        (chosen[:, :, None] == jnp.arange(slot_count, dtype=jnp.int32)[None, None, :]).astype(
            jnp.bfloat16
        ),
        axis=1,
    )
    outgoing = lax.dot_general(
        dispatch, normed, (((0,), (0,)), ((), ())), preferred_element_type=jnp.float32
    )
    outgoing = outgoing.astype(jnp.bfloat16).reshape(ep_count, capacity, local_experts, model_width)
    incoming = lax.all_to_all(outgoing, "ep", split_axis=0, concat_axis=0, tiled=True)
    own_rows = ep_count * capacity
    incoming = incoming.reshape(own_rows, local_experts, model_width)
    hidden_all = joint_hidden(w_gate, w_up, lax.all_gather(incoming, "tp", axis=0, tiled=True))
    summed = lax.psum_scatter(
        joint_down(hidden_all, w_down).astype(jnp.bfloat16), "tp", scatter_dimension=0, tiled=True
    )
    expert_results = summed.reshape(ep_count, capacity, local_experts, model_width)
    returned = lax.all_to_all(
        expert_results, "ep", split_axis=0, concat_axis=0, tiled=True
    ).reshape(slot_count, model_width)
    picked = jnp.take(returned, slot_ids, axis=0).reshape(tok_count, top_count, model_width)
    combined = jnp.sum(route_weights[:, :, None] * picked.astype(jnp.float32), axis=1)
    return combined.astype(jnp.bfloat16)


def body(
    mix_tokens,
    mix_gain,
    w_query,
    w_key,
    w_value,
    query_gain,
    key_gain,
    w_out,
    expert_tokens,
    expert_gain,
    route_ids,
    route_weights,
    w_gate,
    w_up,
    w_down,
):
    mix_out = mixer_half(mix_tokens, mix_gain, w_query, w_key, w_value, query_gain, key_gain, w_out)
    experts_out = expert_half(
        expert_tokens, expert_gain, route_ids, route_weights, w_gate, w_up, w_down
    )
    return (mix_out, experts_out)


def solution(mesh):
    placed = (
        P(("ep", "tp"), None, None),
        P(),
        P(),
        P(),
        P(),
        P(),
        P(),
        P(),
        P(("ep", "tp"), None),
        P(),
        P(("ep", "tp"), None),
        P(("ep", "tp"), None),
        P("ep", None, "tp"),
        P("ep", None, "tp"),
        P("ep", "tp", None),
    )
    return jax.shard_map(
        body,
        mesh=mesh,
        in_specs=placed,
        out_specs=(P(("ep", "tp"), None, None), P(("ep", "tp"), None)),
        check_vma=False,
    )
```

profile of v0, /device:TPU:0, one launch (start us, length us, event | category | flops | bytes accessed | tf_op | source)
XLA Modules:
  0.0 184.7 jit_solution(13140126193179946681)
XLA Ops:
  9.6 1.3 compare_and_fusion
  10.9 1.1 fusion.24
  12.0 1.3 convolution_convert_fusion.1
  13.6 14.4 %all_to_all.43 = bf16[4,36,2,1024]{3,2,1,0:T(2,128)(2,1)S(1)} all-to-all(bf16[4,36,2,1024]{3,2,1,0:T(2,128)(2,1)S(1)} %reshape.608), channel_id=1, replica_groups=mesh['ep'=4,'tp'=8] {'ep'}, dimensions={0} | all-to-all | bytes 1179648 | tf_op jit(solution)/shard_map/all_to_all | solution.py:170
  29.0 50.9 %all-gather.2.cloned.1.call-done = bf16[1152,2,1024]{2,0,1:T(8,128)(2,1)} async-done(((bf16[144,2,1024]{2,0,1:T(8,128)(2,1)}), bf16[1152,2,1024]{2,0,1:T(8,128)(2,1)}) %all-gather.2.cloned.1.call-update) | async-done | bytes 4718608 | tf_op jit(solution)/shard_map/all_gather | solution.py:173
  79.8 7.9 %fusion.56 = f32[2,1152,512]{2,1,0:T(8,128)} fusion(bf16[1152,2,1024]{2,0,1:T(8,128)(2,1)} %all-gather.2.cloned.1.call-done, bf16[2,1024,512]{2,1,0:T(8,128)(2,1)} %param.29), kind=kOutput, calls=%fused_computation.122 | convolution fusion | flops 2415919104 | bytes 11534336 | tf_op jit(solution)/shard_map/rjd,jdf->rjf/dot_general | solution.py:130
  87.7 9.6 %fusion.20 = bf16[1152,2,1024]{2,0,1:T(8,128)(2,1)} fusion(bf16[2,512,1024]{2,1,0:T(8,128)(2,1)S(1)} %copy-done, f32[2,1152,512]{2,1,0:T(8,128)} %fusion.56, bf16[1152,2,1024]{2,0,1:T(8,128)(2,1)} %all-gather.2.cloned.1.call-done, bf16[2,1024,512]{2,1,0:T(8,128)(2,1)} %param.30), kind=kOutput, calls=%fused_computation.31 | convolution fusion | flops 4841275392 | bytes 18350080 | tf_op jit(solution)/shard_map/rjf,jfd->rjd/dot_general | solution.py:136
  99.3 2.1 %fusion.22 = bf16[8,8,8,128]{3,1,2,0:T(8,128)(2,1)S(1)} fusion(bf16[1024,1024]{1,0:T(8,128)(2,1)} %param.19, bf16[64,1,1024]{2,0,1:T(8,128)(2,1)S(1)} %copy-done.2, f32[1024]{0:T(1024)S(1)} %copy-done.6, f32[64]{0:T(128)S(1)} %add_rsqrt_fusion.3), kind=kOutput, calls=%fused_computation.36 | convolution fusion | flops 134545408 | bytes 2363648 | tf_op jit(solution)/shard_map/dot_general | solution.py:87
  102.2 3.4 %all-to-all-start = ((bf16[64,1,8,256]{3,0,1,2:T(8,128)(2,1)}), bf16[64,1,8,256]{3,0,1,2:T(8,128)(2,1)S(1)}, u32[]{:S(2)}, u32[]{:S(2)}) async-start(bf16[64,1,8,256]{3,0,1,2:T(8,128)(2,1)} %pad_maximum_fusion), calls=%async_computation | async-start | bytes 524288 | tf_op jit(solution)/shard_map/all_to_all | solution.py:100
  108.1 11.8 %all-to-all-done = bf16[64,1,8,256]{3,0,1,2:T(8,128)(2,1)S(1)} async-done(((bf16[64,1,8,256]{3,0,1,2:T(8,128)(2,1)}), bf16[64,1,8,256]{3,0,1,2:T(8,128)(2,1)S(1)}, u32[]{:S(2)}, u32[]{:S(2)}) %all-to-all-start) | async-done | bytes 262176 | tf_op jit(solution)/shard_map/all_to_all | solution.py:100
  123.4 10.0 %all_gather.6 = bf16[2048,1,128]{2,0,1:T(8,128)(2,1)S(1)} all-gather(bf16[512,1,128]{2,0,1:T(8,128)(2,1)S(1)} %pad_maximum_fusion.1), channel_id=1, replica_groups=mesh['ep'=4,'tp'=8] {'ep'}, dimensions={0}, use_global_device_ids=true | all-gather | bytes 655360 | tf_op jit(solution)/shard_map/all_gather | solution.py:118
  135.2 14.4 %while.15 = (s32[]{:T(128)}, f32[512,1,2]{0,2,1:T(2,128)S(1)}, f32[512,1,2]{0,2,1:T(2,128)S(1)}, f32[512,1,2,64]{0,3,2,1:T(8,128)S(1)}, bf16[2,1024,1,128]{3,1,0...) while((s32[]{:T(128)}, f32[512,1,2]{0,2,1:T(2,128)S(1)}, ...), condition=%wide.region_6.7_spmd.clone, body=%wide.region_3.6_spmd.clone.sunk | while | flops 277026816 | bytes 31391872 | solution.py:77
  135.4 2.7 %bitcast_reduce_fusion.2 = (f32[512,2]{0,1:T(2,128)S(1)}, f32[1024,512,2]{1,0,2:T(8,128)}) fusion(bf16[512,1,2,64]{0,3,2,1:T(8,128)(2,1)S(1)} %get-tuple-element.182, bf16[1024,1,128]{0,2,1:T(8,128)(2,1)S(1)} %bitcast.161), kind=kOutput, calls=%fused_computation.2.clone.1 | convolution fusion | flops 136313856 | bytes 4460544 | tf_op jit(solution)/shard_map/while/body/eval_jaxpr/qshd,ksd->qshk/dot_general | solution.py:62
  138.1 3.3 %fusion.74 = f32[512,1,2,64]{0,3,2,1:T(8,128)S(1)} fusion(f32[1024,512,2]{1,0,2:T(8,128)} %get-tuple-element.159, f32[512,2]{0,1:T(2,128)S(1)} %bitcast.169, f32[512,1,2,64]{0,3,2,1:T(8,128)S(1)} %get-tuple-element.172, bf16[1024,1,128]{0,2,1:T(8,128)(2,1)S(1)} %bitcast.162, f32[512,2]{0,1:T(2,128)S(1)} %get-tuple-element.160, pred[]{:T(512)S(6)} %compare.47), kind=kOutput, calls=%fused_computation.9.clone.1 | convolution fusion | flops 137560064 | bytes 4857857 | tf_op jit(solution)/shard_map/while/body/eval_jaxpr/qshk,ksd->qshd/dot_general | solution.py:69
  142.6 2.8 %bitcast_reduce_fusion.2 = (f32[512,2]{0,1:T(2,128)S(1)}, f32[1024,512,2]{1,0,2:T(8,128)}) fusion(bf16[512,1,2,64]{0,3,2,1:T(8,128)(2,1)S(1)} %get-tuple-element.182, bf16[1024,1,128]{0,2,1:T(8,128)(2,1)S(1)} %bitcast.161), kind=kOutput, calls=%fused_computation.2.clone.1 | convolution fusion | flops 136313856 | bytes 4460544 | tf_op jit(solution)/shard_map/while/body/eval_jaxpr/qshd,ksd->qshk/dot_general | solution.py:62
  145.3 3.3 %fusion.74 = f32[512,1,2,64]{0,3,2,1:T(8,128)S(1)} fusion(f32[1024,512,2]{1,0,2:T(8,128)} %get-tuple-element.159, f32[512,2]{0,1:T(2,128)S(1)} %bitcast.169, f32[512,1,2,64]{0,3,2,1:T(8,128)S(1)} %get-tuple-element.172, bf16[1024,1,128]{0,2,1:T(8,128)(2,1)S(1)} %bitcast.162, f32[512,2]{0,1:T(2,128)S(1)} %get-tuple-element.160, pred[]{:T(512)S(6)} %compare.47), kind=kOutput, calls=%fused_computation.9.clone.1 | convolution fusion | flops 137560064 | bytes 4857857 | tf_op jit(solution)/shard_map/while/body/eval_jaxpr/qshk,ksd->qshd/dot_general | solution.py:69
  151.6 3.6 %all-to-all-start.1 = ((bf16[8,2,4096]{2,1,0:T(2,128)(2,1)}), bf16[8,2,4096]{2,1,0:T(2,128)(2,1)S(1)}, u32[]{:S(2)}, u32[]{:S(2)}) async-start(bf16[8,2,4096]{2,1,0:T(2,128)(2,1)} %reshape.630), calls=%async_computation.1 | async-start | bytes 262144 | tf_op jit(solution)/shard_map/all_to_all | solution.py:125
  156.2 2.5 %copy.129 = bf16[144,2,1024]{2,1,0:T(2,128)(2,1)} copy(bf16[144,2,1024]{2,0,1:T(8,128)(2,1)} %reduce-scatter.2.cloned.1.call-done) | data formatting | bytes 1179648 | tf_op jit(solution)/shard_map/reduce_scatter | solution.py:174
  158.7 3.0 %all-to-all-done.1 = bf16[8,2,4096]{2,1,0:T(2,128)(2,1)S(1)} async-done(((bf16[8,2,4096]{2,1,0:T(2,128)(2,1)}), bf16[8,2,4096]{2,1,0:T(2,128)(2,1)S(1)}, u32[]{:S(2)}, u32[]{:S(2)}) %all-to-all-start.1) | async-done | bytes 131104 | tf_op jit(solution)/shard_map/all_to_all | solution.py:125
  161.7 3.5 %all-to-all-start.3 = ((bf16[4,36,2,1024]{3,2,1,0:T(2,128)(2,1)}), bf16[4,36,2,1024]{3,2,1,0:T(2,128)(2,1)S(1)}, u32[]{:S(2)}, u32[]{:S(2)}) async-start(bf16[4,36,2,1024]{3,2,1,0:T(2,128)(2,1)} %bitcast.25), calls=%async_computation.4 | async-start | bytes 1179648 | tf_op jit(solution)/shard_map/all_to_all | solution.py:178
  166.4 2.7 %fusion.23 = bf16[64,1,1024]{2,0,1:T(8,128)(2,1)} fusion(bf16[1024,1024]{1,0:T(8,128)(2,1)} %param.24, bf16[8,8,8,128]{3,2,1,0:T(8,128)(2,1)S(1)} %bitcast.177), kind=kOutput, calls=%fused_computation.37 | convolution fusion | flops 134283264 | bytes 2359296 | tf_op jit(solution)/shard_map/dot_general | solution.py:126
  169.2 4.7 %all-to-all-done.3 = bf16[4,36,2,1024]{3,2,1,0:T(2,128)(2,1)S(1)} async-done(((bf16[4,36,2,1024]{3,2,1,0:T(2,128)(2,1)}), bf16[4,36,2,1024]{3,2,1,0:T(2,128)(2,1)S(1)}, u32[]{:S(2)}, u32[]{:S(2)}) %all-to-all-start.3) | async-done | bytes 589856 | tf_op jit(solution)/shard_map/all_to_all | solution.py:178
  174.1 1.2 gather_fusion
  175.5 2.4 %multiply_reduce_fusion = bf16[128,1024]{1,0:T(8,128)(2,1)} fusion(bf16[128,2,1024]{2,1,0:T(2,128)(2,1)S(1)} %gather.7, pred[128,2]{1,0:T(8,128)(4,1)S(1)} %copy.127, f32[128,2]{1,0:T(8,128)S(1)} %copy.123), kind=kLoop, calls=%fused_computation.40 | loop fusion | flops 917504 | bytes 787712 | tf_op jit(solution)/shard_map/reduce_sum | solution.py:182
  (110 shorter events, 20.9 us)
Async XLA Ops:
  7.2 80.6 %copy-start = (bf16[2,512,1024]{2,1,0:T(8,128)(2,1)S(1)}, bf16[2,512,1024]{2,1,0:T(8,128)(2,1)}, u32[]{:S(2)}) copy-start(bf16[2,512,1024]{2,1,0:T(8,128)(2,1)} %param.31) | copy-start | bytes 6291460
  7.2 72.7 %all-gather.2.cloned.1.call-start = ((), (), s32[]{:S(2)}) async-start(), calls=%async_computation.5 | async-start | bytes 5308416 | tf_op jit(solution)/shard_map/all_gather | solution.py:173
  8.2 3.8 %copy-start.3 = (s32[128,2]{1,0:T(8,128)}, s32[128,2]{1,0:T(8,128)S(1)}, u32[]{:S(2)}) copy-start(s32[128,2]{1,0:T(8,128)S(1)} %copy.124) | copy-start | bytes 3076
  28.9 127.3 %reduce-scatter.2.cloned.1.call-start = ((), (), s32[]{:S(2)}) async-start(), calls=%async_computation.6 | async-start | bytes 5308416 | tf_op jit(solution)/shard_map/reduce_scatter | solution.py:174
  97.3 0.9 copy-start.2
  97.3 1.1 copy-start.4
  97.3 1.1 copy-start.6
  97.3 1.5 copy-start.5
  98.2 7.5 %copy-start.9 = (f32[64]{0:T(128)S(1)}, f32[64]{0:T(128)}, u32[]{:S(2)}) copy-start(f32[64]{0:T(128)} %param.22) | copy-start | bytes 772
  98.2 8.2 %copy-start.10 = (f32[64]{0:T(128)S(1)}, f32[64]{0:T(128)}, u32[]{:S(2)}) copy-start(f32[64]{0:T(128)} %param.23) | copy-start | bytes 772
  102.2 17.6 %all-to-all-start = ((bf16[64,1,8,256]{3,0,1,2:T(8,128)(2,1)}), bf16[64,1,8,256]{3,0,1,2:T(8,128)(2,1)S(1)}, u32[]{:S(2)}, u32[]{:S(2)}) async-start(bf16[64,1,8,256]{3,0,1,2:T(8,128)(2,1)} %pad_maximum_fusion), calls=%async_computation | async-start | bytes 524288 | tf_op jit(solution)/shard_map/all_to_all | solution.py:100
  105.7 14.2 %copy-start.7 = (f32[16]{0:T(128)}, f32[16]{0:T(128)S(1)}, u32[]{:S(2)}) copy-start(f32[16]{0:T(128)S(1)} %multiply_power_fusion) | copy-start | bytes 196
  135.1 30.1 %copy-start.8 = (pred[128,2]{0,1:T(4,128)(4,1)S(1)}, pred[128,2]{0,1:T(4,128)(4,1)}, u32[]{:S(2)}) copy-start(pred[128,2]{0,1:T(4,128)(4,1)} %get-tuple-element.102) | copy-start | bytes 772
  138.1 3.5 %copy-start.1 = (f32[1024,512,2]{1,0,2:T(8,128)S(1)}, f32[1024,512,2]{1,0,2:T(8,128)}, u32[]{:S(2)}) copy-start(f32[1024,512,2]{1,0,2:T(8,128)} %get-tuple-element.159) | copy-start | bytes 12582916 | tf_op jit(solution)/shard_map/while
  145.3 3.5 %copy-start.1 = (f32[1024,512,2]{1,0,2:T(8,128)S(1)}, f32[1024,512,2]{1,0,2:T(8,128)}, u32[]{:S(2)}) copy-start(f32[1024,512,2]{1,0,2:T(8,128)} %get-tuple-element.159) | copy-start | bytes 12582916 | tf_op jit(solution)/shard_map/while
  151.6 10.1 %all-to-all-start.1 = ((bf16[8,2,4096]{2,1,0:T(2,128)(2,1)}), bf16[8,2,4096]{2,1,0:T(2,128)(2,1)S(1)}, u32[]{:S(2)}, u32[]{:S(2)}) async-start(bf16[8,2,4096]{2,1,0:T(2,128)(2,1)} %reshape.630), calls=%async_computation.1 | async-start | bytes 262144 | tf_op jit(solution)/shard_map/all_to_all | solution.py:125
  161.7 12.2 %all-to-all-start.3 = ((bf16[4,36,2,1024]{3,2,1,0:T(2,128)(2,1)}), bf16[4,36,2,1024]{3,2,1,0:T(2,128)(2,1)S(1)}, u32[]{:S(2)}, u32[]{:S(2)}) async-start(bf16[4,36,2,1024]{3,2,1,0:T(2,128)(2,1)} %bitcast.25), calls=%async_computation.4 | async-start | bytes 1179648 | tf_op jit(solution)/shard_map/all_to_all | solution.py:178
Sparse Core Ops, SparseCore 0:
  29.1 50.7 all-gather.1
  97.5 57.8 reduce-scatter.1
where the time goes:
time: 185 us
  waiting for transfers between devices  70.4 us (38%)
  matrix products  36.2 us (20%)
  blocking collectives  24.4 us (13%)
  local copies, waits for them, and re-layouts  14.9 us (8%)
  between operations  14.5 us (8%)
  other arithmetic  13.7 us (7%)
  starting transfers between devices  10.5 us (6%)
    all_gather x1, waiting for transfers between devices, expert_half(): lax.all_gather(incoming, 'tp', axis=0, tiled=True)  50.9 us
    all_to_all x1, blocking collectives, expert_half(): lax.all_to_all(outgoing, 'ep', split_axis=0, concat_axis=0, tiled=True)  14.4 us
    all_to_all x1, waiting for transfers between devices, mixer_half(): lax.all_to_all(packed, 'tp', split_axis=2, concat_axis=0, tiled=True)  11.8 us
    all_gather x1, blocking collectives, mixer_half(): lax.all_gather(key_pairs, 'ep', axis=0, tiled=True)  10 us
    dot_general x1, matrix products, joint_down(): jnp.einsum('rjf,jfd->rjd', hidden_all, w_down, preferred_element_type=jnp...  9.59 us
    dot_general x1, matrix products, joint_hidden(): jnp.einsum('rjd,jdf->rjf', piece_rows, w_gate, preferred_element_type=jnp...  7.88 us
    dot_general x2, matrix products, step_block(): jnp.einsum('qshk,ksd->qshd', raised.astype(jnp.bfloat16), values_part, pr...  6.52 us
    dot_general x2, matrix products, step_block(): jnp.einsum('qshd,ksd->qshk', queries, keys_part, preferred_element_type=j...  5.5 us
  transfers between devices with their start and end apart: 5, of which 4 were waited for; matrix products, arithmetic and copies ran while one was open for 19% of the time, Pallas kernels for 0%

commit v1 on v0

--- a/solution.py
+++ b/solution.py
@@ -3,6 +3,8 @@
 import jax
 import jax.numpy as jnp
 from jax import lax
+from jax.experimental import pallas as pl
+from jax.experimental.pallas import tpu as pltpu
 from jax.sharding import PartitionSpec as P
 
 HEAD = 64
@@ -77,7 +79,7 @@
     return lax.scan(step_block, fold_state, blocks)[0]
 
 
-def mixer_half(mix_tokens, mix_gain, w_query, w_key, w_value, query_gain, key_gain, w_out):
+def mixer_front(mix_tokens, mix_gain, w_query, w_key, w_value, query_gain, key_gain):
     tp_count = lax.axis_size("tp")
     seq_rows, sequences, model_width = mix_tokens.shape
     head_count = w_query.shape[1] // HEAD
@@ -109,13 +111,19 @@
     own_keys = normalize(arrived[:, :, 0, query_width : query_width + HEAD], key_gain)
     own_keys = turn(own_keys, cosine_table, sine_table).astype(jnp.bfloat16)
     key_pairs = jnp.concatenate([own_keys, arrived[:, :, 0, query_width + HEAD :]], axis=-1)
+    return own_queries, lax.all_gather(key_pairs, "ep", axis=0, tiled=True)
+
+
+def mixer_back(own_queries, all_pairs, w_out):
+    span_rows, sequences, local_heads, _ = own_queries.shape
+    query_width = local_heads * HEAD
     start_state = (
         jnp.full((span_rows, sequences, local_heads), -1e30, jnp.float32),
         jnp.zeros((span_rows, sequences, local_heads), jnp.float32),
         jnp.zeros((span_rows, sequences, local_heads, HEAD), jnp.float32),
     )
     running_max, totals, accumulated = attend(
-        own_queries, start_state, lax.all_gather(key_pairs, "ep", axis=0, tiled=True)
+        own_queries, start_state, all_pairs
     )
     mixed = (
         (accumulated / totals[..., None])
@@ -126,24 +134,42 @@
     return jnp.dot(returned, w_out, preferred_element_type=jnp.float32).astype(jnp.bfloat16)
 
 
-def joint_hidden(w_gate, w_up, piece_rows):
-    gate_act = jnp.einsum("rjd,jdf->rjf", piece_rows, w_gate, preferred_element_type=jnp.float32)
-    up_act = jnp.einsum("rjd,jdf->rjf", piece_rows, w_up, preferred_element_type=jnp.float32)
-    return (jax.nn.silu(gate_act) * up_act).astype(jnp.bfloat16)
-
-
-def joint_down(hidden_all, w_down):
-    group_sum = jnp.einsum(
-        "rjf,jfd->rjd", hidden_all, w_down, preferred_element_type=jnp.float32
-    ).astype(jnp.bfloat16)
-    return lax.optimization_barrier(group_sum).astype(jnp.float32)
-
-
-def expert_half(expert_tokens, expert_gain, route_ids, route_weights, w_gate, w_up, w_down):
+def expert_kernel(rows_ref, gate_ref, up_ref, down_ref, sums_ref):
+    rows = rows_ref[0]
+    gate_act = jnp.dot(rows, gate_ref[0], preferred_element_type=jnp.float32)
+    up_act = jnp.dot(rows, up_ref[0], preferred_element_type=jnp.float32)
+    hidden = (gate_act / (1.0 + jnp.exp(-gate_act)) * up_act).astype(jnp.bfloat16)
+    sums_ref[0] = jnp.dot(hidden, down_ref[0], preferred_element_type=jnp.float32).astype(
+        jnp.bfloat16
+    )
+
+
+def expert_sums(rows, w_gate, w_up, w_down):
+    experts, row_count, model_width = rows.shape
+    hidden_units = w_gate.shape[2]
+    block_rows = math.gcd(row_count, 384)
+    row_spec = pl.BlockSpec((1, block_rows, model_width), lambda e, r: (e, r, 0))
+    in_spec = pl.BlockSpec((1, model_width, hidden_units), lambda e, r: (e, 0, 0))
+    return pl.pallas_call(
+        expert_kernel,
+        grid=(experts, row_count // block_rows),
+        in_specs=[
+            row_spec,
+            in_spec,
+            in_spec,
+            pl.BlockSpec((1, hidden_units, model_width), lambda e, r: (e, 0, 0)),
+        ],
+        out_specs=row_spec,
+        out_shape=jax.ShapeDtypeStruct(rows.shape, jnp.bfloat16),
+        compiler_params=pltpu.CompilerParams(vmem_limit_bytes=60 * 1024 * 1024),
+        name="experts",
+    )(rows, w_gate, w_up, w_down)
+
+
+def route_rows(expert_tokens, expert_gain, route_ids, local_experts):
     ep_count = lax.axis_size("ep")
     tok_count, model_width = expert_tokens.shape
     top_count = route_ids.shape[1]
-    local_experts = w_gate.shape[0]
     expert_count = local_experts * ep_count
     capacity = tok_count * top_count * 9 // (8 * expert_count)
     slot_count = ep_count * capacity * local_experts
@@ -170,9 +196,18 @@
     incoming = lax.all_to_all(outgoing, "ep", split_axis=0, concat_axis=0, tiled=True)
     own_rows = ep_count * capacity
     incoming = incoming.reshape(own_rows, local_experts, model_width)
-    hidden_all = joint_hidden(w_gate, w_up, lax.all_gather(incoming, "tp", axis=0, tiled=True))
+    return lax.all_gather(incoming, "tp", axis=0, tiled=True), slot_ids
+
+
+def expert_half(all_rows, slot_ids, route_weights, capacity, w_gate, w_up, w_down):
+    ep_count = lax.axis_size("ep")
+    tok_count, top_count = route_weights.shape
+    local_experts = w_gate.shape[0]
+    model_width = all_rows.shape[-1]
+    slot_count = ep_count * capacity * local_experts
+    group_sums = expert_sums(all_rows.transpose(1, 0, 2), w_gate, w_up, w_down)
     summed = lax.psum_scatter(
-        joint_down(hidden_all, w_down).astype(jnp.bfloat16), "tp", scatter_dimension=0, tiled=True
+        group_sums.transpose(1, 0, 2), "tp", scatter_dimension=0, tiled=True
     )
     expert_results = summed.reshape(ep_count, capacity, local_experts, model_width)
     returned = lax.all_to_all(
@@ -200,10 +235,16 @@
     w_up,
     w_down,
 ):
-    mix_out = mixer_half(mix_tokens, mix_gain, w_query, w_key, w_value, query_gain, key_gain, w_out)
-    experts_out = expert_half(
-        expert_tokens, expert_gain, route_ids, route_weights, w_gate, w_up, w_down
-    )
+    tok_count, top_count = route_ids.shape
+    local_experts = w_gate.shape[0]
+    capacity = tok_count * top_count * 9 // (8 * local_experts * lax.axis_size("ep"))
+    all_rows, slot_ids = route_rows(expert_tokens, expert_gain, route_ids, local_experts)
+    own_queries, all_pairs = mixer_front(
+        mix_tokens, mix_gain, w_query, w_key, w_value, query_gain, key_gain
+    )
+    all_rows, all_pairs = lax.optimization_barrier((all_rows, all_pairs))
+    experts_out = expert_half(all_rows, slot_ids, route_weights, capacity, w_gate, w_up, w_down)
+    mix_out = mixer_back(own_queries, all_pairs, w_out)
     return (mix_out, experts_out)
 
 

time: 185 us -> 179 us (0.968)
  matrix products: 36.2 us -> 19.2 us
  Pallas kernels: 0 us -> 12.8 us
  waiting for transfers between devices: 70.4 us -> 68.1 us
    all_gather x1, waiting for transfers between devices: 50.9 us -> 20.1 us  [route_rows(): return (lax.all_gather(incoming, 'tp', axis=0, tiled=True), slot_ids)]
    reduce_scatter x1, waiting for transfers between devices: 0.02 us -> 28.8 us  [expert_half(): lax.psum_scatter(group_sums.transpose(1, 0, 2), 'tp', scatter_dimension=0...]
    dot_general x7 -> x5, matrix products: 24.1 us -> 7.19 us  [the longest x1 2.73 us: mixer_back(): jnp.dot(returned, w_out, preferred_element_type=jnp.float32)]
    pallas_call x0 -> x1, Pallas kernels: none -> 12.8 us  [expert_sums(): pl.pallas_call(expert_kernel, grid=(experts, row_count // block_rows), in...]
where the time goes in v1:
time: 179 us; the launch traced here: 178 us
  waiting for transfers between devices  68.1 us (38%)
  blocking collectives  24.1 us (13%)
  matrix products  19.2 us (11%)
  local copies, waits for them, and re-layouts  15.2 us (8%)
  between operations  14.5 us (8%)
  Pallas kernels  12.8 us (7%)
  other arithmetic  12.1 us (7%)
  starting transfers between devices  12 us (7%)
    reduce_scatter x1, waiting for transfers between devices, expert_half(): lax.psum_scatter(group_sums.transpose(1, 0, 2), 'tp', scatter_dimension=0...  28.8 us
    all_gather x1, waiting for transfers between devices, route_rows(): return (lax.all_gather(incoming, 'tp', axis=0, tiled=True), slot_ids)  20.1 us
    all_to_all x1, waiting for transfers between devices, mixer_front(): lax.all_to_all(packed, 'tp', split_axis=2, concat_axis=0, tiled=True)  16.1 us
    all_to_all x1, blocking collectives, route_rows(): lax.all_to_all(outgoing, 'ep', split_axis=0, concat_axis=0, tiled=True)  14.4 us
    pallas_call x1, Pallas kernels, expert_sums(): pl.pallas_call(expert_kernel, grid=(experts, row_count // block_rows), in...  12.8 us
    all_gather x1, blocking collectives, mixer_front(): return (own_queries, lax.all_gather(key_pairs, 'ep', axis=0, tiled=True))  9.75 us
    dot_general x2, matrix products, step_block(): jnp.einsum('qshk,ksd->qshd', raised.astype(jnp.bfloat16), values_part, pr...  6.51 us
    dot_general x2, matrix products, step_block(): jnp.einsum('qshd,ksd->qshk', queries, keys_part, preferred_element_type=j...  5.5 us
  transfers between devices with their start and end apart: 5, of which 4 were waited for; matrix products, arithmetic and copies ran while one was open for 19% of the time, Pallas kernels for 0%

profile of v1, /device:TPU:0, one launch (start us, length us, event | category | flops | bytes accessed | tf_op | source)
XLA Modules:
  0.0 178.1 jit_solution(15463338279017733982)
XLA Ops:
  9.6 1.3 compare_and_fusion
  12.1 1.3 convolution_convert_fusion
  13.7 14.4 %all_to_all.43 = bf16[4,36,2,1024]{3,2,1,0:T(2,128)(2,1)S(1)} all-to-all(bf16[4,36,2,1024]{3,2,1,0:T(2,128)(2,1)S(1)} %reshape.598), channel_id=1, replica_groups=mesh['ep'=4,'tp'=8] {'ep'}, dimensions={0} | all-to-all | bytes 1179648 | tf_op jit(solution)/shard_map/all_to_all | solution.py:196
  29.2 1.3 convolution_convert_fusion.4
  30.6 1.3 convolution_convert_fusion.3
  33.5 4.9 %all-to-all-start.1 = ((bf16[64,1,8,256]{3,0,1,2:T(8,128)(2,1)}), bf16[64,1,8,256]{3,0,1,2:T(8,128)(2,1)S(1)}, u32[]{:S(2)}, u32[]{:S(2)}) async-start(bf16[64,1,8,256]{3,0,1,2:T(8,128)(2,1)} %pad_maximum_fusion), calls=%async_computation.1 | async-start | bytes 524288 | tf_op jit(solution)/shard_map/all_to_all | solution.py:102
  38.5 16.1 %all-to-all-done.1 = bf16[64,1,8,256]{3,0,1,2:T(8,128)(2,1)S(1)} async-done(((bf16[64,1,8,256]{3,0,1,2:T(8,128)(2,1)}), bf16[64,1,8,256]{3,0,1,2:T(8,128)(2,1)S(1)}, u32[]{:S(2)}, u32[]{:S(2)}) %all-to-all-start.1) | async-done | bytes 262176 | tf_op jit(solution)/shard_map/all_to_all | solution.py:102
  55.7 9.8 %all_gather.7 = bf16[2048,1,128]{2,0,1:T(8,128)(2,1)S(1)} all-gather(bf16[512,1,128]{2,0,1:T(8,128)(2,1)S(1)} %pad_maximum_fusion.1), channel_id=1, replica_groups=mesh['ep'=4,'tp'=8] {'ep'}, dimensions={0}, use_global_device_ids=true | all-gather | bytes 655360 | tf_op jit(solution)/shard_map/all_gather | solution.py:114
  65.5 20.1 %all-gather.2.cloned.1.call-done = bf16[1152,2,1024]{2,0,1:T(8,128)(2,1)} async-done(((bf16[144,2,1024]{2,0,1:T(8,128)(2,1)}), bf16[1152,2,1024]{2,0,1:T(8,128)(2,1)}) %all-gather.2.cloned.1.call-update) | async-done | bytes 4718608 | tf_op jit(solution)/shard_map/all_gather | solution.py:199
  85.5 12.8 %experts.1 = bf16[2,1152,1024]{2,1,0:T(8,128)(2,1)} custom-call(bf16[2,1152,1024]{2,1,0:T(8,128)(2,1)} %bitcast.140, bf16[2,1024,512]{2,1,0:T(8,128)(2,1)} %gate_ref.1, bf16[2,1024,512]{2,1,0:T(8,128)(2,1)} %up_ref.1, bf16[2,512,1024]{2,1,0:T(8,128)(2,1)} %down_ref.1), custom_call_target="tpu_custom_call" | custom-call | tf_op jit(solution)/shard_map/experts/pallas_call | solution.py:153
  102.5 1.1 copy.122
  104.5 14.4 %while.15 = (s32[]{:T(128)}, f32[512,1,2]{0,2,1:T(2,128)S(1)}, f32[512,1,2]{0,2,1:T(2,128)S(1)}, f32[512,1,2,64]{0,3,2,1:T(8,128)S(1)}, bf16[2,1024,1,128]{3,1,0...) while((s32[]{:T(128)}, f32[512,1,2]{0,2,1:T(2,128)S(1)}, ...), condition=%wide.region_11.12_spmd.clone, body=%wide.region_8.11_spmd.clone.sunk | while | flops 277026816 | bytes 31391872 | solution.py:79
  104.7 2.7 %bitcast_reduce_fusion.2 = (f32[512,2]{0,1:T(2,128)S(1)}, f32[1024,512,2]{1,0,2:T(8,128)}) fusion(bf16[512,1,2,64]{0,3,2,1:T(8,128)(2,1)S(1)} %get-tuple-element.186, bf16[1024,1,128]{0,2,1:T(8,128)(2,1)S(1)} %bitcast.135), kind=kOutput, calls=%fused_computation.2.clone.1 | convolution fusion | flops 136313856 | bytes 4460544 | tf_op jit(solution)/shard_map/while/body/eval_jaxpr/qshd,ksd->qshk/dot_general | solution.py:64
  107.5 3.2 %fusion.61 = f32[512,1,2,64]{0,3,2,1:T(8,128)S(1)} fusion(f32[1024,512,2]{1,0,2:T(8,128)} %get-tuple-element.163, f32[512,2]{0,1:T(2,128)S(1)} %bitcast.145, f32[512,1,2,64]{0,3,2,1:T(8,128)S(1)} %get-tuple-element.176, bf16[1024,1,128]{0,2,1:T(8,128)(2,1)S(1)} %bitcast.136, f32[512,2]{0,1:T(2,128)S(1)} %get-tuple-element.164, pred[]{:T(512)S(6)} %compare.47), kind=kOutput, calls=%fused_computation.9.clone.1 | convolution fusion | flops 137560064 | bytes 4857857 | tf_op jit(solution)/shard_map/while/body/eval_jaxpr/qshk,ksd->qshd/dot_general | solution.py:71
  111.9 2.7 %bitcast_reduce_fusion.2 = (f32[512,2]{0,1:T(2,128)S(1)}, f32[1024,512,2]{1,0,2:T(8,128)}) fusion(bf16[512,1,2,64]{0,3,2,1:T(8,128)(2,1)S(1)} %get-tuple-element.186, bf16[1024,1,128]{0,2,1:T(8,128)(2,1)S(1)} %bitcast.135), kind=kOutput, calls=%fused_computation.2.clone.1 | convolution fusion | flops 136313856 | bytes 4460544 | tf_op jit(solution)/shard_map/while/body/eval_jaxpr/qshd,ksd->qshk/dot_general | solution.py:64
  114.6 3.3 %fusion.61 = f32[512,1,2,64]{0,3,2,1:T(8,128)S(1)} fusion(f32[1024,512,2]{1,0,2:T(8,128)} %get-tuple-element.163, f32[512,2]{0,1:T(2,128)S(1)} %bitcast.145, f32[512,1,2,64]{0,3,2,1:T(8,128)S(1)} %get-tuple-element.176, bf16[1024,1,128]{0,2,1:T(8,128)(2,1)S(1)} %bitcast.136, f32[512,2]{0,1:T(2,128)S(1)} %get-tuple-element.164, pred[]{:T(512)S(6)} %compare.47), kind=kOutput, calls=%fused_computation.9.clone.1 | convolution fusion | flops 137560064 | bytes 4857857 | tf_op jit(solution)/shard_map/while/body/eval_jaxpr/qshk,ksd->qshd/dot_general | solution.py:71
  121.0 3.4 %all-to-all-start.2 = ((bf16[8,2,4096]{2,1,0:T(2,128)(2,1)}), bf16[8,2,4096]{2,1,0:T(2,128)(2,1)S(1)}, u32[]{:S(2)}, u32[]{:S(2)}) async-start(bf16[8,2,4096]{2,1,0:T(2,128)(2,1)} %reshape.627), calls=%async_computation.2 | async-start | bytes 262144 | tf_op jit(solution)/shard_map/all_to_all | solution.py:133
  125.3 28.8 %reduce-scatter.2.cloned.1.call-done = bf16[144,2,1024]{2,0,1:T(8,128)(2,1)} async-done(((bf16[1152,2,1024]{2,0,1:T(8,128)(2,1)}), bf16[144,2,1024]{2,0,1:T(8,128)(2,1)}) %reduce-scatter.2.cloned.1.call-update) | async-done | bytes 589840 | tf_op jit(solution)/shard_map/reduce_scatter | solution.py:209
  154.1 2.5 %copy.129 = bf16[144,2,1024]{2,1,0:T(2,128)(2,1)} copy(bf16[144,2,1024]{2,0,1:T(8,128)(2,1)} %reduce-scatter.2.cloned.1.call-done) | data formatting | bytes 1179648 | tf_op jit(solution)/shard_map/reduce_scatter | solution.py:209
  156.6 3.7 %all-to-all-start.3 = ((bf16[4,36,2,1024]{3,2,1,0:T(2,128)(2,1)}), bf16[4,36,2,1024]{3,2,1,0:T(2,128)(2,1)S(1)}, u32[]{:S(2)}, u32[]{:S(2)}) async-start(bf16[4,36,2,1024]{3,2,1,0:T(2,128)(2,1)} %bitcast.24), calls=%async_computation.4 | async-start | bytes 1179648 | tf_op jit(solution)/shard_map/all_to_all | solution.py:213
  161.5 2.7 %fusion.17 = bf16[64,1,1024]{2,0,1:T(8,128)(2,1)} fusion(bf16[1024,1024]{1,0:T(8,128)(2,1)} %param.24, bf16[8,8,8,128]{3,2,1,0:T(8,128)(2,1)S(1)} %bitcast.153), kind=kOutput, calls=%fused_computation.27 | convolution fusion | flops 134283264 | bytes 2359296 | tf_op jit(solution)/shard_map/dot_general | solution.py:134
  164.2 3.0 %all-to-all-done.3 = bf16[4,36,2,1024]{3,2,1,0:T(2,128)(2,1)S(1)} async-done(((bf16[4,36,2,1024]{3,2,1,0:T(2,128)(2,1)}), bf16[4,36,2,1024]{3,2,1,0:T(2,128)(2,1)S(1)}, u32[]{:S(2)}, u32[]{:S(2)}) %all-to-all-start.3) | async-done | bytes 589856 | tf_op jit(solution)/shard_map/all_to_all | solution.py:213
  167.5 1.2 gather_fusion
  168.9 2.4 %multiply_reduce_fusion = bf16[128,1024]{1,0:T(8,128)(2,1)} fusion(bf16[128,2,1024]{2,1,0:T(2,128)(2,1)S(1)} %gather.7, pred[128,2]{1,0:T(8,128)(4,1)S(1)} %copy.128, f32[128,2]{1,0:T(8,128)S(1)} %copy.127), kind=kLoop, calls=%fused_computation.30 | loop fusion | flops 917504 | bytes 787712 | tf_op jit(solution)/shard_map/reduce_sum | solution.py:217
  (103 shorter events, 19.6 us)
Async XLA Ops:
  7.2 24.9 %copy-start = (bf16[1024,1024]{1,0:T(8,128)(2,1)S(1)}, bf16[1024,1024]{1,0:T(8,128)(2,1)}, u32[]{:S(2)}) copy-start(bf16[1024,1024]{1,0:T(8,128)(2,1)} %param.19) | copy-start | bytes 6291460
  7.2 21.8 %copy-start.2 = (bf16[64,1,1024]{2,0,1:T(8,128)(2,1)S(1)}, bf16[64,1,1024]{2,0,1:T(8,128)(2,1)}, u32[]{:S(2)}) copy-start(bf16[64,1,1024]{2,0,1:T(8,128)(2,1)} %param.17) | copy-start | bytes 393220
  7.2 22.0 %copy-start.4 = (f32[1024]{0:T(1024)S(1)}, f32[1024]{0:T(1024)}, u32[]{:S(2)}) copy-start(f32[1024]{0:T(1024)} %param.18) | copy-start | bytes 12292
  7.2 78.3 %all-gather.2.cloned.1.call-start = ((), (), s32[]{:S(2)}) async-start(), calls=%async_computation.5 | async-start | bytes 5308416 | tf_op jit(solution)/shard_map/all_gather | solution.py:199
  8.2 3.9 %copy-start.3 = (s32[128,2]{1,0:T(8,128)}, s32[128,2]{1,0:T(8,128)S(1)}, u32[]{:S(2)}) copy-start(s32[128,2]{1,0:T(8,128)S(1)} %copy.114) | copy-start | bytes 3076
  28.0 10.4 %copy-start.6 = (f32[64]{0:T(128)S(1)}, f32[64]{0:T(128)}, u32[]{:S(2)}) copy-start(f32[64]{0:T(128)} %param.23) | copy-start | bytes 772
  33.5 21.2 %all-to-all-start.1 = ((bf16[64,1,8,256]{3,0,1,2:T(8,128)(2,1)}), bf16[64,1,8,256]{3,0,1,2:T(8,128)(2,1)S(1)}, u32[]{:S(2)}, u32[]{:S(2)}) async-start(bf16[64,1,8,256]{3,0,1,2:T(8,128)(2,1)} %pad_maximum_fusion), calls=%async_computation.1 | async-start | bytes 524288 | tf_op jit(solution)/shard_map/all_to_all | solution.py:102
  38.3 115.8 %reduce-scatter.2.cloned.1.call-start = ((), (), s32[]{:S(2)}) async-start(), calls=%async_computation.6 | async-start | bytes 5308416 | tf_op jit(solution)/shard_map/reduce_scatter | solution.py:209
  98.3 0.7 copy-start.7
  104.5 55.8 %copy-start.5 = (pred[128,2]{0,1:T(4,128)(4,1)S(1)}, pred[128,2]{0,1:T(4,128)(4,1)}, u32[]{:S(2)}) copy-start(pred[128,2]{0,1:T(4,128)(4,1)} %get-tuple-element.106) | copy-start | bytes 772
  107.4 3.5 %copy-start.1 = (f32[1024,512,2]{1,0,2:T(8,128)S(1)}, f32[1024,512,2]{1,0,2:T(8,128)}, u32[]{:S(2)}) copy-start(f32[1024,512,2]{1,0,2:T(8,128)} %get-tuple-element.163) | copy-start | bytes 12582916 | tf_op jit(solution)/shard_map/while
  114.6 3.6 %copy-start.1 = (f32[1024,512,2]{1,0,2:T(8,128)S(1)}, f32[1024,512,2]{1,0,2:T(8,128)}, u32[]{:S(2)}) copy-start(f32[1024,512,2]{1,0,2:T(8,128)} %get-tuple-element.163) | copy-start | bytes 12582916 | tf_op jit(solution)/shard_map/while
  121.0 35.7 %all-to-all-start.2 = ((bf16[8,2,4096]{2,1,0:T(2,128)(2,1)}), bf16[8,2,4096]{2,1,0:T(2,128)(2,1)S(1)}, u32[]{:S(2)}, u32[]{:S(2)}) async-start(bf16[8,2,4096]{2,1,0:T(2,128)(2,1)} %reshape.627), calls=%async_computation.2 | async-start | bytes 262144 | tf_op jit(solution)/shard_map/all_to_all | solution.py:133
  156.6 10.6 %all-to-all-start.3 = ((bf16[4,36,2,1024]{3,2,1,0:T(2,128)(2,1)}), bf16[4,36,2,1024]{3,2,1,0:T(2,128)(2,1)S(1)}, u32[]{:S(2)}, u32[]{:S(2)}) async-start(bf16[4,36,2,1024]{3,2,1,0:T(2,128)(2,1)} %bitcast.24), calls=%async_computation.4 | async-start | bytes 1179648 | tf_op jit(solution)/shard_map/all_to_all | solution.py:213
Sparse Core Ops, SparseCore 0:
  29.1 56.3 all-gather.1
  98.5 55.6 reduce-scatter.1
